TPU v7x, 512 devices: a 4x2x32 block of a 4x8x32 slice. The times are simulated.
512 devices in a mesh: grp: 2 (over y), sp: 32 (over z), tp: 8 (over x, core).
Axes of the slice: x: 4, y: 2, z: 32, core: 2. Of those that a mesh axis runs over, the one named last changes fastest.
The devices are a block of a 4x8x32 slice.
Arguments:
- latent: bfloat16 [32768, 4096], P(('grp', 'sp', 'tp')), parts along dimension 0, may hold values from -260 to 260
- context: bfloat16 [1536, 4096], P(('grp', 'sp')), parts along dimension 0, may hold values from -6 to 6
- conditioning: bfloat16 [8192], P(('grp', 'sp')), parts along dimension 0, may hold values from -6 to 6
- norm_gain: float32 [4096], replicated, may hold values from 0.1 to 1.9
- shift_weight: bfloat16 [4096, 4096], P('sp', 'tp'), may hold values from -0.09375 to 0.09375
- scale_weight: bfloat16 [4096, 4096], P('sp', 'tp'), may hold values from -0.09375 to 0.09375
- gate_weight: bfloat16 [4096, 4096], P('sp', 'tp'), may hold values from -0.09375 to 0.09375
- query_weight: bfloat16 [4096, 1024], P(None, 'tp'), may hold values from -3 to 3
- key_weight: bfloat16 [4096, 512], P(None, 'tp'), may hold values from -3 to 3
- value_weight: bfloat16 [4096, 512], P(None, 'tp'), may hold values from -0.09375 to 0.09375
- out_weight: bfloat16 [1024, 4096], P(None, 'tp'), may hold values from -1.5 to 1.5
- sink_logit: float32 [16], P('tp'), may hold values from 3 to 7
Outputs:
- mixed: bfloat16 [32768, 4096], P(('grp', 'sp', 'tp')), parts along dimension 0
There are 2 independent parts, one for each index of `grp`. A program takes and returns all parts, laid end to end along the dimension named above; an argument that names none is the same for every part. Nothing has to cross between parts.
All inputs are finite; a program needn't handle non-finite values.
Results may differ from a plain program's by a relative error of at most 0.012.
The roundings to bfloat16 on the way count: a program that leaves them out, or rounds other values in their place, can miss the bound.
Values may be sent and summed in bfloat16 or wider, within the bound.
A program may use at most 64 MiB of HBM per device.

v0:
```python
import jax
import jax.numpy as jnp
from jax import lax
from jax.sharding import PartitionSpec as P

HEADS = 16
KV_HEADS = 8
HD = 64
GRID_W = 64
WIN = 128
epsilon = 1e-06
rope_base = 10000.0
neg_large = -1e30


def sent_to_all(value, axis):
    count = lax.axis_size(axis)
    return lax.all_to_all(
        jnp.broadcast_to(value[None], (count, *value.shape)), axis, 0, 0, tiled=True
    )


def over_copies(value, axis):
    return sent_to_all(value, axis).sum(axis=0)


def packed_total(arrays, axis):
    ends = [0]
    for a in arrays:
        ends.append(ends[-1] + a.size)
    running = over_copies(jnp.concatenate([a.ravel() for a in arrays]), axis)
    return tuple((running[b:e].reshape(a.shape) for a, b, e in zip(arrays, ends, ends[1:])))


def rows_first(arrays, axis, dims):
    turned = [jnp.moveaxis(a, dim, 0) for a, dim in zip(arrays, dims)]
    both = jnp.concatenate([t.reshape(len(t), -1) for t in turned], axis=1)
    whole, at, outs = (lax.all_gather(both, axis, axis=0, tiled=True), 0, [])
    for t, dim in zip(turned, dims):
        share = whole[:, at : at + t[0].size].reshape(-1, *t.shape[1:])
        outs.append(jnp.moveaxis(share, 0, dim))
        at += t[0].size
    return tuple(outs)


def with_halo(cells, sides, width):
    for axis, dim in sides:
        count = lax.axis_size(axis)
        ends = count - 1
        head = lax.slice_in_dim(cells, 0, width, axis=dim)
        tail = lax.slice_in_dim(cells, cells.shape[dim] - width, cells.shape[dim], axis=dim)
        cells = jnp.concatenate(
            [
                lax.ppermute(tail, axis, [(i, (i + 1) % count) for i in range(ends)]),
                cells,
                lax.ppermute(head, axis, [((i + 1) % count, i) for i in range(ends)]),
            ],
            axis=dim,
        )
    return cells


def laid_out(tiles, dim):
    shape = list(tiles.shape[1:])
    shape[dim] *= tiles.shape[0]
    return jnp.moveaxis(tiles, 0, dim).reshape(shape)


def collect(value, axis, dim):
    return laid_out(sent_to_all(value, axis), dim)


def row_norm(matrix, norm_gain):
    values = matrix.astype(jnp.float32)
    return (
        values * lax.rsqrt(jnp.mean(values * values, axis=-1, keepdims=True) + epsilon) * norm_gain
    )


def axial_turn(values, position):
    half_dim = values.shape[-1] // 2
    quarter = half_dim // 2
    inverse = rope_base ** (-jnp.arange(quarter, dtype=jnp.float32) / quarter)

    def turn(section, coordinate):
        angles = coordinate.astype(jnp.float32)[:, None] * inverse[None, :]
        cosine = jnp.cos(angles)[:, None, :]
        sine_part = jnp.sin(angles)[:, None, :]
        leading = section[..., :quarter]
        trailing = section[..., quarter:]
        return jnp.concatenate(
            [leading * cosine - trailing * sine_part, leading * sine_part + trailing * cosine],
            axis=-1,
        )

    return jnp.concatenate(
        [
            turn(values[..., :half_dim], position // GRID_W),
            turn(values[..., half_dim:], position % GRID_W),
        ],
        axis=-1,
    )


def context_pairs(context_rows, norm_gain, key_weight, value_weight):
    prepared = row_norm(context_rows, norm_gain).astype(jnp.bfloat16)
    return jnp.concatenate(
        [
            jnp.dot(prepared, key_weight, preferred_element_type=jnp.float32),
            jnp.dot(prepared, value_weight, preferred_element_type=jnp.float32),
        ],
        axis=1,
    ).astype(jnp.bfloat16)


def local(
    latent,
    context,
    conditioning,
    norm_gain,
    shift_weight,
    scale_weight,
    gate_weight,
    query_weight,
    key_weight,
    value_weight,
    out_weight,
    sink_logit,
):
    lifted = jax.nn.silu(conditioning.astype(jnp.float32)).astype(jnp.bfloat16)[None, :]
    shift_part = jnp.dot(lifted, shift_weight, preferred_element_type=jnp.float32)[0]
    scale_part = jnp.dot(lifted, scale_weight, preferred_element_type=jnp.float32)[0]
    gate_part = jnp.dot(lifted, gate_weight, preferred_element_type=jnp.float32)[0]
    summed = packed_total((shift_part, scale_part, gate_part), "sp")
    shift_vec, scale_vec, gate_vec = rows_first((summed[0], summed[1], summed[2]), "tp", (0, 0, 0))
    normed = (row_norm(latent, norm_gain) * (1.0 + scale_vec) + shift_vec).astype(jnp.bfloat16)
    segment = lax.all_gather(normed, "tp", axis=0, tiled=True)
    projected = jnp.concatenate(
        [
            jnp.dot(segment, query_weight, preferred_element_type=jnp.float32),
            jnp.dot(segment, key_weight, preferred_element_type=jnp.float32),
            jnp.dot(segment, value_weight, preferred_element_type=jnp.float32),
        ],
        axis=1,
    )
    row_count = projected.shape[0]
    query_width = query_weight.shape[1]
    key_width = key_weight.shape[1]
    query_heads = query_width // HD
    pair_heads = key_width // HD
    group_size = HEADS // KV_HEADS
    row_offset = lax.axis_index("sp") * row_count
    position = row_offset + jnp.arange(row_count, dtype=jnp.int32)
    queries = axial_turn(
        projected[:, :query_width].reshape(row_count, query_heads, HD), position
    ).astype(jnp.bfloat16)
    latent_keys = axial_turn(
        projected[:, query_width : query_width + key_width].reshape(row_count, pair_heads, HD),
        position,
    ).astype(jnp.bfloat16)
    latent_values = projected[:, query_width + key_width :].astype(jnp.bfloat16)
    key_value = jnp.concatenate([latent_keys.reshape(row_count, key_width), latent_values], axis=1)
    widened = with_halo(key_value, (("sp", 0),), WIN)
    context_all = collect(context_pairs(context, norm_gain, key_weight, value_weight), "sp", 0)
    block_count = row_count // WIN
    context_count = context_all.shape[0]
    query_blocks = queries.reshape(block_count, WIN, pair_heads, group_size, HD)
    band_blocks = widened.reshape(block_count + 2, WIN, 2 * key_width)
    band_rows = jnp.concatenate(
        [band_blocks[:block_count], band_blocks[1 : block_count + 1], band_blocks[2:]], axis=1
    )
    band_keys = band_rows[..., :key_width].reshape(block_count, 3 * WIN, pair_heads, HD)
    band_values = band_rows[..., key_width:].reshape(block_count, 3 * WIN, pair_heads, HD)
    context_keys = context_all[:, :key_width].reshape(context_count, pair_heads, HD)
    context_values = context_all[:, key_width:].reshape(context_count, pair_heads, HD)
    factor = HD ** (-0.5)
    local_scores = (
        jnp.einsum("nqhgd,nkhd->nhgqk", query_blocks, band_keys, preferred_element_type=jnp.float32)
        * factor
    )
    query_pos = position.reshape(block_count, WIN)
    key_pos = (
        row_offset
        - WIN
        + jnp.arange(block_count, dtype=jnp.int32)[:, None] * WIN
        + jnp.arange(3 * WIN, dtype=jnp.int32)[None, :]
    )
    seq_total = row_count * lax.axis_size("sp")
    allowed = (
        (jnp.abs(key_pos[:, None, :] - query_pos[:, :, None]) <= WIN)
        & (key_pos[:, None, :] >= 0)
        & (key_pos[:, None, :] < seq_total)
    )
    local_scores = jnp.where(allowed[:, None, None], local_scores, neg_large)
    context_scores = (
        jnp.einsum(
            "nqhgd,thd->nhgqt", query_blocks, context_keys, preferred_element_type=jnp.float32
        )
        * factor
    )
    sink_values = sink_logit.reshape(pair_heads, group_size)[None, :, :, None, None]
    highest = jnp.maximum(
        jnp.maximum(
            jnp.max(local_scores, axis=-1, keepdims=True),
            jnp.max(context_scores, axis=-1, keepdims=True),
        ),
        sink_values,
    )
    local_exp = jnp.exp(local_scores - highest)
    context_exp = jnp.exp(context_scores - highest)
    denominator = (
        jnp.sum(local_exp, axis=-1, keepdims=True)
        + jnp.sum(context_exp, axis=-1, keepdims=True)
        + jnp.exp(sink_values - highest)
    )
    local_weights = (local_exp / denominator).astype(jnp.bfloat16)
    context_weights = (context_exp / denominator).astype(jnp.bfloat16)
    attended = jnp.einsum(
        "nhgqk,nkhd->nqhgd", local_weights, band_values, preferred_element_type=jnp.float32
    ) + jnp.einsum(
        "nhgqt,thd->nqhgd", context_weights, context_values, preferred_element_type=jnp.float32
    )
    attended = attended.reshape(row_count, query_width).astype(jnp.bfloat16)
    columns_part = jnp.dot(
        collect(attended, "tp", 1), out_weight, preferred_element_type=jnp.float32
    ).astype(jnp.bfloat16)
    blended = lax.all_to_all(columns_part, "tp", split_axis=0, concat_axis=1, tiled=True)
    return (latent.astype(jnp.float32) + gate_vec * blended.astype(jnp.float32)).astype(
        jnp.bfloat16
    )


def solution(mesh):
    in_specs = (
        P(("grp", "sp", "tp"), None),
        P(("grp", "sp"), None),
        P(("grp", "sp")),
        P(),
        P("sp", "tp"),
        P("sp", "tp"),
        P("sp", "tp"),
        P(None, "tp"),
        P(None, "tp"),
        P(None, "tp"),
        P(None, "tp"),
        P("tp"),
    )
    out_specs = P(("grp", "sp", "tp"), None)
    return jax.shard_map(local, mesh=mesh, in_specs=in_specs, out_specs=out_specs, check_vma=False)
```

profile of v0, /device:TPU:33, one launch (start us, length us, event | category | flops | bytes accessed | tf_op | source)
XLA Modules:
  0.0 197.6 jit_solution(16965403692785830598)
XLA Ops:
  6.6 1.2 fusion.60
  7.8 1.1 fusion.58
  8.8 1.1 fusion.56
  9.9 0.8 broadcast_in_dim.14
  10.7 46.3 %all-to-all-start = ((f32[32,1,1536]{2,1,0:T(1,128)}), f32[32,1,1536]{2,1,0:T(1,128)S(1)}, u32[]{:S(2)}, u32[]{:S(2)}) async-start(f32[32,1,1536]{2,1,0:T(1,128)} %broadcast_in_dim.14), calls=%async_computation | async-start | bytes 393216 | tf_op jit(solution)/shard_map/all_to_all | solution.py:18
  57.1 1.2 fusion.12
  58.3 33.6 %all-to-all-done = f32[32,1,1536]{2,1,0:T(1,128)S(1)} async-done(((f32[32,1,1536]{2,1,0:T(1,128)}), f32[32,1,1536]{2,1,0:T(1,128)S(1)}, u32[]{:S(2)}, u32[]{:S(2)}) %all-to-all-start) | async-done | bytes 196640 | tf_op jit(solution)/shard_map/all_to_all | solution.py:18
  92.0 15.7 %all_gather.6 = f32[4096,3]{0,1:T(4,128)S(1)} all-gather(f32[512,3]{0,1:T(4,128)S(1)} %pad_maximum_fusion.3), channel_id=1, replica_groups=mesh['grp'=2,'sp'=32,'tp'=8] {'tp'}, dimensions={0}, use_global_device_ids=true | all-gather | bytes 55296 | tf_op jit(solution)/shard_map/all_gather | solution.py:38
  107.8 2.1 %fusion.16 = bf16[64,4096]{1,0:T(8,128)(2,1)} fusion(bf16[64,4096]{1,0:T(8,128)(2,1)} %param.12, f32[4096]{0:T(1024)S(1)} %bitcast.164, f32[4096]{0:T(1024)S(1)} %bitcast.165, f32[4096]{0:T(1024)} %param.15, f32[64]{0:T(128)S(1)} %add_rsqrt_fusion.1), kind=kLoop, calls=%fused_computation.29 | loop fusion | flops 1572864 | bytes 1097984 | tf_op jit(solution)/shard_map/convert_element_type | solution.py:136
  110.9 0.7 broadcast_in_dim.17
  111.6 4.8 %all-to-all-start.1 = ((bf16[32,24,128]{2,1,0:T(8,128)(2,1)}), bf16[32,24,128]{2,1,0:T(8,128)(2,1)S(1)}, u32[]{:S(2)}, u32[]{:S(2)}) async-start(bf16[32,24,128]{2,1,0:T(8,128)(2,1)} %broadcast_in_dim.17), calls=%async_computation.1 | async-start | bytes 393216 | tf_op jit(solution)/shard_map/all_to_all | solution.py:18
  116.9 0.9 fusion.20
  117.9 21.9 %all-gather.2.cloned.1.call-done = bf16[512,4096]{1,0:T(8,128)(2,1)} async-done(((bf16[64,4096]{1,0:T(8,128)(2,1)}), bf16[512,4096]{1,0:T(8,128)(2,1)}) %all-gather.2.cloned.1.call-update) | async-done | bytes 4194320 | tf_op jit(solution)/shard_map/all_gather | solution.py:137
  139.8 3.7 %convolution_bitcast_fusion.1 = f32[512,1,64]{0,2,1:T(8,128)S(1)} fusion(bf16[512,4096]{1,0:T(8,128)(2,1)} %all-gather.2.cloned.1.call-done, bf16[4096,64]{0,1:T(8,128)(2,1)S(1)} %copy-done.3), kind=kOutput, calls=%fused_computation.20 | convolution fusion | flops 268435456 | bytes 4849664 | tf_op jit(solution)/shard_map/dot_general | solution.py:141
  144.3 1.4 fusion.11
  145.7 1.3 collective-permute-start.1
  147.0 4.2 %collective-permute-start = (bf16[128,128]{0,1:T(8,128)(2,1)S(1)}, bf16[128,128]{0,1:T(8,128)(2,1)S(1)}, u32[]{:S(2)}, u32[]{:S(2)}) collective-permute-start(bf16[128,128]{0,1:T(8,128)(2,1)S(1)} %get-tuple-element.14), channel_id=1, source_target_pairs={{0,8},{8,16},{16,24},{24,32},{32,40},{40,48},{48,56},{56,64},{64,7... | collective-permute-start | bytes 98312 | tf_op jit(solution)/shard_map/ppermute | solution.py:54
  151.3 1.5 fusion.70
  152.9 0.6 bitcast_reduce_fusion
  155.1 0.8 fusion.7
  156.5 19.3 %all_to_all.29 = bf16[8,512,128]{1,2,0:T(8,128)(2,1)S(1)} all-to-all(bf16[8,512,128]{1,2,0:T(8,128)(2,1)S(1)} %broadcast_in_dim.18), channel_id=1, replica_groups=mesh['grp'=2,'sp'=32,'tp'=8] {'tp'}, dimensions={0} | all-to-all | bytes 2097152 | tf_op jit(solution)/shard_map/all_to_all | solution.py:18
  175.9 0.7 convolution_convert_fusion
  176.6 13.0 %all_to_all.30 = bf16[8,64,512]{2,1,0:T(8,128)(2,1)S(1)} all-to-all(bf16[8,64,512]{2,1,0:T(8,128)(2,1)S(1)} %bitcast.161), channel_id=1, replica_groups=mesh['grp'=2,'sp'=32,'tp'=8] {'tp'}, dimensions={0} | all-to-all | bytes 1048576 | tf_op jit(solution)/shard_map/all_to_all | solution.py:227
  189.8 0.9 fusion.17
  (66 shorter events, 5.0 us)
Async XLA Ops:
  6.5 169.3 %copy-start = (bf16[1024,512]{1,0:T(8,128)(2,1)S(1)}, bf16[1024,512]{1,0:T(8,128)(2,1)}, u32[]{:S(2)}) copy-start(bf16[1024,512]{1,0:T(8,128)(2,1)} %param.22) | copy-start | bytes 3145732
  6.6 103.6 %copy-start.7 = (f32[4096]{0:T(1024)S(1)}, f32[4096]{0:T(1024)}, u32[]{:S(2)}) copy-start(f32[4096]{0:T(1024)} %param.15) | copy-start | bytes 49156
  6.6 103.4 %copy-start.5 = (bf16[24,4096]{1,0:T(8,128)(2,1)S(1)}, bf16[24,4096]{1,0:T(8,128)(2,1)}, u32[]{:S(2)}) copy-start(bf16[24,4096]{1,0:T(8,128)(2,1)} %param.13) | copy-start | bytes 589828
  6.6 103.6 %copy-start.4 = (bf16[4096,64]{0,1:T(8,128)(2,1)S(1)}, bf16[4096,64]{0,1:T(8,128)(2,1)}, u32[]{:S(2)}) copy-start(bf16[4096,64]{0,1:T(8,128)(2,1)} %param.21) | copy-start | bytes 1572868
  6.6 103.9 %copy-start.3 = (bf16[4096,64]{0,1:T(8,128)(2,1)S(1)}, bf16[4096,64]{0,1:T(8,128)(2,1)}, u32[]{:S(2)}) copy-start(bf16[4096,64]{0,1:T(8,128)(2,1)} %param.20) | copy-start | bytes 1572868
  10.7 81.2 %all-to-all-start = ((f32[32,1,1536]{2,1,0:T(1,128)}), f32[32,1,1536]{2,1,0:T(1,128)S(1)}, u32[]{:S(2)}, u32[]{:S(2)}) async-start(f32[32,1,1536]{2,1,0:T(1,128)} %broadcast_in_dim.14), calls=%async_computation | async-start | bytes 393216 | tf_op jit(solution)/shard_map/all_to_all | solution.py:18
  57.0 82.8 %all-gather.2.cloned.1.call-start = ((), (), s32[]{:S(2)}) async-start(), calls=%async_computation.4 | async-start | bytes 4718592 | tf_op jit(solution)/shard_map/all_gather | solution.py:137
  111.6 41.3 %all-to-all-start.1 = ((bf16[32,24,128]{2,1,0:T(8,128)(2,1)}), bf16[32,24,128]{2,1,0:T(8,128)(2,1)S(1)}, u32[]{:S(2)}, u32[]{:S(2)}) async-start(bf16[32,24,128]{2,1,0:T(8,128)(2,1)} %broadcast_in_dim.17), calls=%async_computation.1 | async-start | bytes 393216 | tf_op jit(solution)/shard_map/all_to_all | solution.py:18
  139.8 4.5 %copy-start.1 = (bf16[512,4096]{1,0:T(8,128)(2,1)S(1)}, bf16[512,4096]{1,0:T(8,128)(2,1)}, u32[]{:S(2)}) copy-start(bf16[512,4096]{1,0:T(8,128)(2,1)} %all-gather.2.cloned.1.call-done) | copy-start | bytes 12582916
  143.5 7.8 %copy-start.6 = (bf16[4096,128]{1,0:T(8,128)(2,1)S(1)}, bf16[4096,128]{1,0:T(8,128)(2,1)}, u32[]{:S(2)}) copy-start(bf16[4096,128]{1,0:T(8,128)(2,1)} %param.19) | copy-start | bytes 3145732
  145.7 7.8 %collective-permute-start.1 = (bf16[128,128]{0,1:T(8,128)(2,1)S(1)}, bf16[128,128]{0,1:T(8,128)(2,1)S(1)}, u32[]{:S(2)}, u32[]{:S(2)}) collective-permute-start(bf16[128,128]{0,1:T(8,128)(2,1)S(1)} %get-tuple-element.13), channel_id=1, source_target_pairs={{8,0},{16,8},{24,16},{32,24},{40,32},{48,40},{56,48},{64,56},{72,6... | collective-permute-start | bytes 98312 | tf_op jit(solution)/shard_map/ppermute | solution.py:56
  147.0 6.5 %collective-permute-start = (bf16[128,128]{0,1:T(8,128)(2,1)S(1)}, bf16[128,128]{0,1:T(8,128)(2,1)S(1)}, u32[]{:S(2)}, u32[]{:S(2)}) collective-permute-start(bf16[128,128]{0,1:T(8,128)(2,1)S(1)} %get-tuple-element.14), channel_id=1, source_target_pairs={{0,8},{8,16},{16,24},{24,32},{32,40},{40,48},{48,56},{56,64},{64,7... | collective-permute-start | bytes 98312 | tf_op jit(solution)/shard_map/ppermute | solution.py:54
  152.9 1.2 copy-start.8
  176.6 13.2 %copy-start.2 = (bf16[64,4096]{1,0:T(8,128)(2,1)S(1)}, bf16[64,4096]{1,0:T(8,128)(2,1)}, u32[]{:S(2)}) copy-start(bf16[64,4096]{1,0:T(8,128)(2,1)} %param.12) | copy-start | bytes 1572868
Sparse Core Ops, SparseCore 0:
  110.1 29.6 all-gather.1
where the time goes:
time: 198 us
  starting transfers between devices  56.7 us (29%)
  waiting for transfers between devices  55.5 us (28%)
  blocking collectives  48 us (24%)
  between operations  13.8 us (7%)
  matrix products  13.5 us (7%)
  other arithmetic  8.05 us (4%)
  local copies, waits for them, and re-layouts  2.02 us (1%)
    all_to_all x2, starting transfers between devices, sent_to_all(): lax.all_to_all(jnp.broadcast_to(value[None], (count, *value.shape)), axis...  51.1 us
    all_to_all x2, waiting for transfers between devices, sent_to_all(): lax.all_to_all(jnp.broadcast_to(value[None], (count, *value.shape)), axis...  33.6 us
    all_gather x1, waiting for transfers between devices, local(): segment = lax.all_gather(normed, 'tp', axis=0, tiled=True)  21.9 us
    all_to_all x1, blocking collectives, sent_to_all(): lax.all_to_all(jnp.broadcast_to(value[None], (count, *value.shape)), axis...  19.3 us
    all_gather x1, blocking collectives, rows_first(): whole, at, outs = (lax.all_gather(both, axis, axis=0, tiled=True), 0, [])  15.7 us
    all_to_all x1, blocking collectives, local(): lax.all_to_all(columns_part, 'tp', split_axis=0, concat_axis=1, tiled=True)  13 us
    ppermute x1, starting transfers between devices, with_halo(): lax.ppermute(tail, axis, [(i, (i + 1) % count) for i in range(ends)])  4.21 us
  transfers between devices with their start and end apart: 5, of which 2 were waited for; matrix products, arithmetic and copies ran while one was open for 6% of the time, Pallas kernels for 0%

commit v1 on v0

--- a/solution.py
+++ b/solution.py
@@ -134,7 +134,11 @@
     summed = packed_total((shift_part, scale_part, gate_part), "sp")
     shift_vec, scale_vec, gate_vec = rows_first((summed[0], summed[1], summed[2]), "tp", (0, 0, 0))
     normed = (row_norm(latent, norm_gain) * (1.0 + scale_vec) + shift_vec).astype(jnp.bfloat16)
-    segment = lax.all_gather(normed, "tp", axis=0, tiled=True)
+    size = lax.axis_size("tp")
+    repeats = [size if d == 0 else 1 for d in range(normed.ndim)]
+    segment = lax.all_to_all(
+        jnp.tile(normed, repeats), "tp", split_axis=0, concat_axis=0, tiled=True
+    )
     projected = jnp.concatenate(
         [
             jnp.dot(segment, query_weight, preferred_element_type=jnp.float32),

time: 198 us -> 238 us (1.20)
  waiting for transfers between devices: 55.5 us -> 97.3 us
  between operations: 13.8 us -> 0.37 us
  matrix products: 13.5 us -> 17.7 us
  local copies, waits for them, and re-layouts: 2.02 us -> 5.89 us
  starting transfers between devices: 56.7 us -> 59.7 us
    all_to_all x0 -> x1, waiting for transfers between devices: none -> 45.1 us  [local(): lax.all_to_all(jnp.tile(normed, repeats), 'tp', split_axis=0, concat_axis...]
    all_gather x1 -> x0, waiting for transfers between devices: 21.9 us -> none  [local(): segment = lax.all_gather(normed, 'tp', axis=0, tiled=True)]
    all_to_all x2, waiting for transfers between devices: 33.6 us -> 52.2 us  [sent_to_all(): lax.all_to_all(jnp.broadcast_to(value[None], (count, *value.shape)), axis...]
    all_to_all x0 -> x1, starting transfers between devices: none -> 4.75 us  [local(): lax.all_to_all(jnp.tile(normed, repeats), 'tp', split_axis=0, concat_axis...]
    another operation x0 -> x1, local copies, waits for them, and re-layouts: none -> 2.5 us  [local(): jnp.tile(normed, repeats)]
  transfers between devices with their start and end apart: 5 -> 5, of which waited for: 2 -> 3; matrix products, arithmetic and copies ran while one was open for 6% -> 7% of each run, Pallas kernels for 0% -> 0%
where the time goes in v1:
time: 238 us
  waiting for transfers between devices  97.3 us (41%)
  starting transfers between devices  59.7 us (25%)
  blocking collectives  49.4 us (21%)
  matrix products  17.7 us (7%)
  other arithmetic  7.25 us (3%)
  local copies, waits for them, and re-layouts  5.89 us (2%)
    all_to_all x2, waiting for transfers between devices, sent_to_all(): lax.all_to_all(jnp.broadcast_to(value[None], (count, *value.shape)), axis...  52.2 us
    all_to_all x2, starting transfers between devices, sent_to_all(): lax.all_to_all(jnp.broadcast_to(value[None], (count, *value.shape)), axis...  51.1 us
    all_to_all x1, waiting for transfers between devices, local(): lax.all_to_all(jnp.tile(normed, repeats), 'tp', split_axis=0, concat_axis...  45.1 us
    all_to_all x1, blocking collectives, sent_to_all(): lax.all_to_all(jnp.broadcast_to(value[None], (count, *value.shape)), axis...  20.7 us
    all_gather x1, blocking collectives, rows_first(): whole, at, outs = (lax.all_gather(both, axis, axis=0, tiled=True), 0, [])  15.7 us
    all_to_all x1, blocking collectives, local(): lax.all_to_all(columns_part, 'tp', split_axis=0, concat_axis=1, tiled=True)  13 us
  transfers between devices with their start and end apart: 5, of which 3 were waited for; matrix products, arithmetic and copies ran while one was open for 7% of the time, Pallas kernels for 0%

profile of v1, /device:TPU:33, one launch (start us, length us, event | category | flops | bytes accessed | tf_op | source)
XLA Modules:
  0.0 237.6 jit_solution(15978489735749285395)
XLA Ops:
  0.0 1.1 fusion.60
  1.1 1.1 fusion.58
  2.2 1.1 fusion.56
  4.1 46.3 %all-to-all-start = ((f32[32,1,1536]{2,1,0:T(1,128)}), f32[32,1,1536]{2,1,0:T(1,128)S(1)}, u32[]{:S(2)}, u32[]{:S(2)}) async-start(f32[32,1,1536]{2,1,0:T(1,128)} %broadcast_in_dim.14), calls=%async_computation | async-start | bytes 393216 | tf_op jit(solution)/shard_map/all_to_all | solution.py:18
  50.4 1.2 fusion.12
  51.6 33.6 %all-to-all-done = f32[32,1,1536]{2,1,0:T(1,128)S(1)} async-done(((f32[32,1,1536]{2,1,0:T(1,128)}), f32[32,1,1536]{2,1,0:T(1,128)S(1)}, u32[]{:S(2)}, u32[]{:S(2)}) %all-to-all-start) | async-done | bytes 196640 | tf_op jit(solution)/shard_map/all_to_all | solution.py:18
  85.4 15.7 %all_gather.3 = f32[4096,3]{0,1:T(4,128)S(1)} all-gather(f32[512,3]{0,1:T(4,128)S(1)} %pad_maximum_fusion.3), channel_id=1, replica_groups=mesh['grp'=2,'sp'=32,'tp'=8] {'tp'}, dimensions={0}, use_global_device_ids=true | all-gather | bytes 55296 | tf_op jit(solution)/shard_map/all_gather | solution.py:38
  101.2 1.3 fusion.16
  102.5 2.5 %tile.2 = bf16[8,64,4096]{2,1,0:T(8,128)(2,1)} broadcast(bf16[64,4096]{1,0:T(8,128)(2,1)S(1)} %fusion.16), dimensions={1,2} | broadcast | bytes 4718592 | tf_op jit(solution)/shard_map/tile | solution.py:140
  105.0 4.8 %all-to-all-start.1 = ((bf16[8,64,4096]{2,1,0:T(8,128)(2,1)}), bf16[8,64,4096]{2,1,0:T(8,128)(2,1)}, u32[]{:S(2)}, u32[]{:S(2)}) async-start(bf16[8,64,4096]{2,1,0:T(8,128)(2,1)} %tile.2), calls=%async_computation.1 | async-start | bytes 8388608 | tf_op jit(solution)/shard_map/all_to_all | solution.py:139
  109.8 1.4 copy.57
  112.6 0.9 fusion.20
  113.6 45.1 %all-to-all-done.1 = bf16[8,64,4096]{2,1,0:T(8,128)(2,1)} async-done(((bf16[8,64,4096]{2,1,0:T(8,128)(2,1)}), bf16[8,64,4096]{2,1,0:T(8,128)(2,1)}, u32[]{:S(2)}, u32[]{:S(2)}) %all-to-all-start.1) | async-done | bytes 4194336 | tf_op jit(solution)/shard_map/all_to_all | solution.py:139
  159.4 4.8 %all-to-all-start.2 = ((bf16[32,24,128]{2,1,0:T(8,128)(2,1)}), bf16[32,24,128]{2,1,0:T(8,128)(2,1)S(1)}, u32[]{:S(2)}, u32[]{:S(2)}) async-start(bf16[32,24,128]{2,1,0:T(8,128)(2,1)} %broadcast_in_dim.17), calls=%async_computation.2 | async-start | bytes 393216 | tf_op jit(solution)/shard_map/all_to_all | solution.py:18
  164.1 3.6 %convolution_bitcast_fusion.1 = f32[512,1,64]{0,2,1:T(8,128)S(1)} fusion(bf16[512,4096]{1,0:T(8,128)(2,1)} %bitcast.12, bf16[4096,64]{0,1:T(8,128)(2,1)S(1)} %copy-done.2), kind=kOutput, calls=%fused_computation.20 | convolution fusion | flops 268435456 | bytes 4849664 | tf_op jit(solution)/shard_map/dot_general | solution.py:145
  168.5 3.6 %fusion.11 = bf16[512,128]{0,1:T(8,128)(2,1)S(1)} fusion(bf16[512,128]{0,1:T(8,128)(2,1)S(1)} %constant_dynamic-update-slice_fusion, bf16[512,4096]{1,0:T(8,128)(2,1)} %bitcast.12, bf16[4096,64]{0,1:T(8,128)(2,1)S(1)} %copy-done.3), kind=kOutput, calls=%fused_computation.22 | convolution fusion | flops 268468224 | bytes 4784128 | tf_op jit(solution)/shard_map/dot_general | solution.py:146
  172.1 2.4 collective-permute-start
  174.5 1.5 collective-permute-start.1
  176.0 3.7 %fusion.70 = f32[512,2,64]{0,2,1:T(8,128)S(1)} fusion(bf16[512,4096,1]{1,0,2:T(8,128)(2,1)} %bitcast.22, bf16[2,64,4096]{2,1,0:T(8,128)(2,1)S(1)} %bitcast.161), kind=kOutput, calls=%fused_computation.135 | convolution fusion | flops 536870912 | bytes 5505024 | tf_op jit(solution)/shard_map/dot_general | solution.py:144
  179.9 18.6 %all-to-all-done.2 = bf16[32,24,128]{2,1,0:T(8,128)(2,1)S(1)} async-done(((bf16[32,24,128]{2,1,0:T(8,128)(2,1)}), bf16[32,24,128]{2,1,0:T(8,128)(2,1)S(1)}, u32[]{:S(2)}, u32[]{:S(2)}) %all-to-all-start.2) | async-done | bytes 196640 | tf_op jit(solution)/shard_map/all_to_all | solution.py:18
  200.6 0.8 fusion.7
  202.0 20.7 %all_to_all.38 = bf16[8,512,128]{1,2,0:T(8,128)(2,1)S(1)} all-to-all(bf16[8,512,128]{1,2,0:T(8,128)(2,1)S(1)} %broadcast_in_dim.18), channel_id=1, replica_groups=mesh['grp'=2,'sp'=32,'tp'=8] {'tp'}, dimensions={0} | all-to-all | bytes 2097152 | tf_op jit(solution)/shard_map/all_to_all | solution.py:18
  223.5 13.0 %all_to_all.39 = bf16[8,64,512]{2,1,0:T(8,128)(2,1)S(1)} all-to-all(bf16[8,64,512]{2,1,0:T(8,128)(2,1)S(1)} %bitcast.166), channel_id=1, replica_groups=mesh['grp'=2,'sp'=32,'tp'=8] {'tp'}, dimensions={0} | all-to-all | bytes 1048576 | tf_op jit(solution)/shard_map/all_to_all | solution.py:231
  236.7 0.9 fusion.17
  (67 shorter events, 7.6 us)
Async XLA Ops:
  0.0 222.7 %copy-start = (bf16[1024,512]{1,0:T(8,128)(2,1)S(1)}, bf16[1024,512]{1,0:T(8,128)(2,1)}, u32[]{:S(2)}) copy-start(bf16[1024,512]{1,0:T(8,128)(2,1)} %param.22) | copy-start | bytes 3145732
  4.1 81.2 %all-to-all-start = ((f32[32,1,1536]{2,1,0:T(1,128)}), f32[32,1,1536]{2,1,0:T(1,128)S(1)}, u32[]{:S(2)}, u32[]{:S(2)}) async-start(f32[32,1,1536]{2,1,0:T(1,128)} %broadcast_in_dim.14), calls=%async_computation | async-start | bytes 393216 | tf_op jit(solution)/shard_map/all_to_all | solution.py:18
  105.0 4.8 %copy-start.5 = (bf16[4096,128]{1,0:T(8,128)(2,1)S(1)}, bf16[4096,128]{1,0:T(8,128)(2,1)}, u32[]{:S(2)}) copy-start(bf16[4096,128]{1,0:T(8,128)(2,1)} %param.19) | copy-start | bytes 3145732
  105.0 6.2 %copy-start.4 = (bf16[24,4096]{1,0:T(8,128)(2,1)S(1)}, bf16[24,4096]{1,0:T(8,128)(2,1)}, u32[]{:S(2)}) copy-start(bf16[24,4096]{1,0:T(8,128)(2,1)} %param.13) | copy-start | bytes 589828
  105.0 6.4 %copy-start.3 = (bf16[4096,64]{0,1:T(8,128)(2,1)S(1)}, bf16[4096,64]{0,1:T(8,128)(2,1)}, u32[]{:S(2)}) copy-start(bf16[4096,64]{0,1:T(8,128)(2,1)} %param.21) | copy-start | bytes 1572868
  105.0 6.4 %copy-start.7 = (f32[4096]{0:T(1024)S(1)}, f32[4096]{0:T(1024)}, u32[]{:S(2)}) copy-start(f32[4096]{0:T(1024)} %param.15) | copy-start | bytes 49156
  105.0 6.7 %copy-start.2 = (bf16[4096,64]{0,1:T(8,128)(2,1)S(1)}, bf16[4096,64]{0,1:T(8,128)(2,1)}, u32[]{:S(2)}) copy-start(bf16[4096,64]{0,1:T(8,128)(2,1)} %param.20) | copy-start | bytes 1572868
  105.0 53.6 %all-to-all-start.1 = ((bf16[8,64,4096]{2,1,0:T(8,128)(2,1)}), bf16[8,64,4096]{2,1,0:T(8,128)(2,1)}, u32[]{:S(2)}, u32[]{:S(2)}) async-start(bf16[8,64,4096]{2,1,0:T(8,128)(2,1)} %tile.2), calls=%async_computation.1 | async-start | bytes 8388608 | tf_op jit(solution)/shard_map/all_to_all | solution.py:139
  159.4 39.1 %all-to-all-start.2 = ((bf16[32,24,128]{2,1,0:T(8,128)(2,1)}), bf16[32,24,128]{2,1,0:T(8,128)(2,1)S(1)}, u32[]{:S(2)}, u32[]{:S(2)}) async-start(bf16[32,24,128]{2,1,0:T(8,128)(2,1)} %broadcast_in_dim.17), calls=%async_computation.2 | async-start | bytes 393216 | tf_op jit(solution)/shard_map/all_to_all | solution.py:18
  167.7 8.3 %copy-start.6 = (bf16[4096,128]{0,1:T(8,128)(2,1)S(1)}, bf16[4096,128]{0,1:T(8,128)(2,1)}, u32[]{:S(2)}) copy-start(bf16[4096,128]{0,1:T(8,128)(2,1)} %copy.57) | copy-start | bytes 3145732
  172.1 26.9 %collective-permute-start = (bf16[128,128]{0,1:T(8,128)(2,1)S(1)}, bf16[128,128]{0,1:T(8,128)(2,1)S(1)}, u32[]{:S(2)}, u32[]{:S(2)}) collective-permute-start(bf16[128,128]{0,1:T(8,128)(2,1)S(1)} %get-tuple-element.14), channel_id=1, source_target_pairs={{0,8},{8,16},{16,24},{24,32},{32,40},{40,48},{48,56},{56,64},{64,7... | collective-permute-start | bytes 98312 | tf_op jit(solution)/shard_map/ppermute | solution.py:54
  174.5 24.5 %collective-permute-start.1 = (bf16[128,128]{0,1:T(8,128)(2,1)S(1)}, bf16[128,128]{0,1:T(8,128)(2,1)S(1)}, u32[]{:S(2)}, u32[]{:S(2)}) collective-permute-start(bf16[128,128]{0,1:T(8,128)(2,1)S(1)} %get-tuple-element.13), channel_id=1, source_target_pairs={{8,0},{16,8},{24,16},{32,24},{40,32},{48,40},{56,48},{64,56},{72,6... | collective-permute-start | bytes 98312 | tf_op jit(solution)/shard_map/ppermute | solution.py:56
  198.4 1.2 copy-start.8
  223.4 13.2 %copy-start.1 = (bf16[64,4096]{1,0:T(8,128)(2,1)S(1)}, bf16[64,4096]{1,0:T(8,128)(2,1)}, u32[]{:S(2)}) copy-start(bf16[64,4096]{1,0:T(8,128)(2,1)} %param.12) | copy-start | bytes 1572868
